TPU v7x, 32 devices: a whole 2x2x4 slice. The times are simulated.
32 devices in a mesh: sp: 16 (over z, y, x), tp: 2 (over core).
Axes of the slice: x: 2, y: 2, z: 4, core: 2. Of those that a mesh axis runs over, the one named last changes fastest.
Arguments:
- residual: bfloat16 [4096, 2048], P(('sp', 'tp')), may hold values from -6 to 6
- query_nope: bfloat16 [4096, 1024], P('sp', 'tp'), may hold values from -24 to 24
- query_rope: bfloat16 [4096, 512], P('sp', 'tp'), may hold values from -400 to 400
- latent: bfloat16 [4096, 256], P(('sp', 'tp')), may hold values from -6 to 6
- key_rope: bfloat16 [4096, 64], P(('sp', 'tp')), may hold values from -6 to 6
- key_up: bfloat16 [256, 1024], P(None, 'tp'), may hold values from -0.375 to 0.375
- value_up: bfloat16 [256, 1024], P(None, 'tp'), may hold values from -0.375 to 0.375
- out_proj: bfloat16 [1024, 2048], replicated, may hold values from -0.375 to 0.375
- norm_gain: float32 [2048], replicated, may hold values from 0.1 to 1.9
- routes: int32 [4096, 2], P(('sp', 'tp')), may hold values from 0 to 15, all different within a row; in each aligned block of 128 rows (0 to 127, 128 to 255, ...) at most 32 rows name the same one
- route_weight: float32 [4096, 2], P(('sp', 'tp')), may hold values from 0.3 to 2.5
- w_gate: bfloat16 [16, 2048, 512], P('sp', None, 'tp'), may hold values from -0.125 to 0.125
- w_up: bfloat16 [16, 2048, 512], P('sp', None, 'tp'), may hold values from -0.125 to 0.125
- w_down: bfloat16 [16, 512, 2048], P('sp', 'tp'), may hold values from -0.25 to 0.25
Outputs:
- mixed: bfloat16 [4096, 2048], P(('sp', 'tp'))
Inputs may be any that keep to these rules, and one draw needn't show every extreme that they name: `routes`: each row names 2 different experts. Among the rows of one device no expert is named more than 32 times, a bound that some block reaches by the rows of some device.
All inputs are finite; a program needn't handle non-finite values.
Results may differ from a plain program's by a relative error of at most 0.015.
Values may be sent and summed in bfloat16 or wider, within the bound.
A program may use at most 128 MiB of HBM per device.

v0:
```python
import jax
import jax.numpy as jnp
from jax import lax
from jax.sharding import PartitionSpec as P

QK_NOPE = 128
QK_ROPE = 64
V_DIM = 128
SEGMENT = 64
EPSILON = 1e-06
ROPE_BASE = 10000.0
NEG_LARGE = -1e30


def rotary(values, positions):
    half_width = values.shape[-1] // 2
    inverse = ROPE_BASE ** (-2.0 * jnp.arange(half_width, dtype=jnp.float32) / values.shape[-1])
    angles = positions.astype(jnp.float32)[:, None] * inverse[None, :]
    cosine = jnp.cos(angles)
    sine_part = jnp.sin(angles)
    if values.ndim == 3:
        cosine = cosine[:, None, :]
        sine_part = sine_part[:, None, :]
    first_half = values[..., :half_width]
    second = values[..., half_width:]
    return jnp.concatenate(
        [first_half * cosine - second * sine_part, second * cosine + first_half * sine_part],
        axis=-1,
    )


def local(
    residual,
    query_nope,
    query_rope,
    latent,
    key_rope,
    key_up,
    value_up,
    out_proj,
    norm_gain,
    routes,
    route_weight,
    w_gate,
    w_up,
    w_down,
):
    tp_count = lax.axis_size("tp")
    tp_index = lax.axis_index("tp")
    sp_index = lax.axis_index("sp")
    row_count = residual.shape[0]
    tok_dev = query_nope.shape[0]
    heads_here = query_nope.shape[1] // QK_NOPE
    score_scale = (QK_NOPE + QK_ROPE) ** (-0.5)
    query_first = sp_index * tok_dev
    query_pos = query_first + jnp.arange(tok_dev, dtype=jnp.int32)
    query_rot = rotary(
        query_rope.astype(jnp.float32).reshape(tok_dev, heads_here, QK_ROPE), query_pos
    ).astype(jnp.bfloat16)
    query_heads = query_nope.reshape(tok_dev, heads_here, QK_NOPE)
    key_pos = query_first + tp_index * row_count + jnp.arange(row_count, dtype=jnp.int32)
    key_rot = rotary(key_rope.astype(jnp.float32), key_pos).astype(jnp.bfloat16)
    query_segment = query_pos // SEGMENT
    last_segment = (query_first + tok_dev - 1) // SEGMENT
    initial = (
        jnp.full((heads_here, tok_dev), NEG_LARGE, jnp.float32),
        jnp.zeros((heads_here, tok_dev), jnp.float32),
        jnp.zeros((tok_dev, heads_here, V_DIM), jnp.float32),
    )
    paired = (
        lax.all_gather(latent, "tp", axis=0, tiled=True),
        lax.all_gather(key_rot, "tp", axis=0, tiled=True),
    )
    lat_rows = lax.all_gather(paired[0], "sp", axis=0, tiled=True)
    rot_rows = lax.all_gather(paired[1], "sp", axis=0, tiled=True)
    piece_rows = lat_rows.shape[0]
    key_block = piece_rows
    while key_block > 2048 and key_block % 2 == 0:
        key_block //= 2
    block_count = piece_rows // key_block

    def one_block(state_now, inputs):
        lat_block, rot_block, offset = inputs
        key_nope = jnp.dot(lat_block, key_up, preferred_element_type=jnp.float32).astype(
            jnp.bfloat16
        )
        key_nope = key_nope.reshape(key_block, heads_here, QK_NOPE)
        value_rows = jnp.dot(lat_block, value_up, preferred_element_type=jnp.float32).astype(
            jnp.bfloat16
        )
        value_rows = value_rows.reshape(key_block, heads_here, V_DIM)
        scores = jnp.einsum(
            "qhd,khd->hqk", query_heads, key_nope, preferred_element_type=jnp.float32
        )
        scores = (
            scores
            + jnp.einsum("qhr,kr->hqk", query_rot, rot_block, preferred_element_type=jnp.float32)
        ) * score_scale
        key_segment = (offset + jnp.arange(key_block, dtype=jnp.int32)) // SEGMENT
        allowed = (key_segment[None, :] <= query_segment[:, None])[None]
        scores = jnp.where(allowed, scores, NEG_LARGE)
        old_max, old_sum, old_acc = state_now
        new_max = jnp.maximum(old_max, jnp.max(scores, axis=-1))
        weights = jnp.where(allowed, jnp.exp(scores - new_max[:, :, None]), 0.0)
        shrink = jnp.exp(old_max - new_max)
        new_sum = old_sum * shrink + jnp.sum(weights, axis=-1)
        new_acc = old_acc * shrink.T[:, :, None] + jnp.einsum(
            "hqk,khv->qhv",
            weights.astype(jnp.bfloat16),
            value_rows,
            preferred_element_type=jnp.float32,
        )
        return ((new_max, new_sum, new_acc), None)

    def compute(state_now):
        result, unused = lax.scan(
            one_block,
            state_now,
            (
                lat_rows.reshape(block_count, key_block, lat_rows.shape[1]),
                rot_rows.reshape(block_count, key_block, rot_rows.shape[1]),
                jnp.arange(block_count, dtype=jnp.int32) * key_block,
            ),
        )
        return result

    def keep_state(state_now):
        return state_now

    row_max, weight_sum, weighted = lax.cond(
        jnp.int32(0) // SEGMENT <= last_segment, compute, keep_state, initial
    )
    attn_out = (
        (weighted / weight_sum.T[:, :, None])
        .astype(jnp.bfloat16)
        .reshape(tok_dev, heads_here * V_DIM)
    )
    all_heads = lax.all_to_all(attn_out, "tp", split_axis=0, concat_axis=1, tiled=True)
    projected = jnp.dot(all_heads, out_proj, preferred_element_type=jnp.float32)
    hidden_wide = residual.astype(jnp.float32) + projected
    hidden = hidden_wide.astype(jnp.bfloat16)
    hidden_wide = hidden.astype(jnp.float32)
    normed = hidden_wide * lax.rsqrt(
        jnp.mean(hidden_wide * hidden_wide, axis=-1, keepdims=True) + EPSILON
    )
    normed = (normed * norm_gain[None, :]).astype(jnp.bfloat16)
    expert_count = lax.axis_size("sp")
    capacity = max(2, 2 * (row_count * tp_count) // expert_count)
    top_count = routes.shape[1]
    width = normed.shape[1]
    flat_expert = routes.reshape(-1)
    onehot = (flat_expert[:, None] == jnp.arange(expert_count, dtype=jnp.int32)[None, :]).astype(
        jnp.int32
    )
    slot_rank = jnp.sum(jnp.cumsum(onehot, axis=0) * onehot, axis=1) - 1
    slot_index = flat_expert * capacity + slot_rank
    outgoing = (
        jnp.zeros((expert_count * capacity, width), jnp.bfloat16)
        .at[slot_index]
        .set(jnp.repeat(normed, top_count, axis=0))
    )
    gate_weight = w_gate[0]
    up_weight = w_up[0]
    down_weight = w_down[0]
    shard_piece = lax.all_gather(
        lax.all_to_all(
            outgoing.reshape(expert_count, capacity, width),
            "sp",
            split_axis=0,
            concat_axis=0,
            tiled=True,
        ),
        "tp",
        axis=0,
        tiled=True,
    )
    gate_part = jnp.dot(shard_piece, gate_weight, preferred_element_type=jnp.float32)
    up_part = jnp.dot(shard_piece, up_weight, preferred_element_type=jnp.float32)
    activated = (jax.nn.silu(gate_part) * up_part).astype(jnp.bfloat16)
    product = jnp.dot(activated, down_weight, preferred_element_type=jnp.float32)
    summed = lax.psum_scatter(
        lax.optimization_barrier(product.astype(jnp.bfloat16))
        .astype(jnp.float32)
        .astype(jnp.bfloat16),
        "tp",
        scatter_dimension=0,
        tiled=True,
    )
    back_rows = lax.all_to_all(summed, "sp", split_axis=0, concat_axis=0, tiled=True)
    picked = back_rows.reshape(expert_count * capacity, width)[slot_index]
    combined = jnp.sum(
        picked.astype(jnp.float32).reshape(row_count, top_count, width) * route_weight[:, :, None],
        axis=1,
    )
    return (hidden_wide + combined).astype(jnp.bfloat16)


def solution(mesh):
    return jax.shard_map(
        local,
        mesh=mesh,
        in_specs=(
            P(("sp", "tp"), None),
            P("sp", "tp"),
            P("sp", "tp"),
            P(("sp", "tp"), None),
            P(("sp", "tp"), None),
            P(None, "tp"),
            P(None, "tp"),
            P(),
            P(),
            P(("sp", "tp"), None),
            P(("sp", "tp"), None),
            P("sp", None, "tp"),
            P("sp", None, "tp"),
            P("sp", "tp", None),
        ),
        out_specs=P(("sp", "tp"), None),
        check_vma=False,
    )
```

profile of v0, /device:TPU:12, one launch (start us, length us, event | category | flops | bytes accessed | tf_op | source)
XLA Modules:
  0.0 297.6 jit_solution(12448938111200499188)
XLA Ops:
  6.5 3.5 %all_gather.15 = bf16[256,256]{1,0:T(8,128)(2,1)} all-gather(bf16[128,256]{1,0:T(8,128)(2,1)} %param.21), channel_id=1, replica_groups=mesh['sp'=16,'tp'=2] {'tp'}, dimensions={0}, use_global_device_ids=true | all-gather | bytes 196608 | tf_op jit(solution)/shard_map/all_gather | solution.py:71
  14.9 1.9 all_gather.17
  17.1 35.9 %all_gather.18 = bf16[4096,64]{0,1:T(8,128)(2,1)S(1)} all-gather(bf16[256,64]{0,1:T(8,128)(2,1)S(1)} %all_gather.17), channel_id=1, replica_groups=mesh['sp'=16,'tp'=2] {'sp'}, dimensions={0}, use_global_device_ids=true | all-gather | bytes 557056 | tf_op jit(solution)/shard_map/all_gather | solution.py:75
  53.0 20.2 %all-gather.3.cloned.1.call-done = bf16[4096,256]{1,0:T(8,128)(2,1)} async-done(((bf16[256,256]{1,0:T(8,128)(2,1)}), bf16[4096,256]{1,0:T(8,128)(2,1)}) %all-gather.3.cloned.1.call-update) | async-done | bytes 2097168 | tf_op jit(solution)/shard_map/all_gather | solution.py:74
  73.2 44.0 %conditional.1 = (f32[4,256]{1,0:T(4,128)}, f32[256,4,128]{0,2,1:T(8,128)}) conditional(s32[]{:T(128)} %convert_element_type.80, () %tuple.28, (bf16[4096,256]{1,0:T(8,128)(2,1)}, bf16[4096,64]{0,1:T(8,128)(2,1)S(1)}, bf16[256,512]{1,0:T(8,128)(2,1)}, s32[256]{0:T(256)S(1)}, s32[256]{0:T(256)S(1)}, /*index=5*/s32[]{:T(128)}, ...), branch_computations={%region_0.1_spmd, %region_1.6_spmd.clone} | conditional | flops 2439948032 | bytes 85153152 | solution.py:130
  74.6 42.6 %while.20 = (s32[]{:T(128)}, f32[4,256]{1,0:T(4,128)S(1)}, f32[4,256]{1,0:T(4,128)}, f32[256,4,128]{0,2,1:T(8,128)}, s32[2]{0:T(128)S(1)}, /*index=5*/s32[256]{0...) while((s32[]{:T(128)}, f32[4,256]{1,0:T(4,128)S(1)}, ...), condition=%wide.region_5.5_spmd.clone, body=%wide.region_2.4_spmd.clone.sunk | while | flops 2439944192 | bytes 83052784 | solution.py:116
  74.6 2.0 convolution_convert_fusion.5
  76.6 1.3 fusion.95
  79.7 5.5 %fusion.96 = (f32[4,256]{1,0:T(4,128)S(1)}, f32[4,256,2048]{1,2,0:T(8,128)}) fusion(bf16[256,4,64]{0,2,1:T(8,128)(2,1)S(1)} %get-tuple-element.537, bf16[2,2048,64]{1,2,0:T(8,128)(2,1)S(1)} %get-tuple-element.536, s32[]{:T(128)} %get-tuple-element.513, f32[4,2048,256]{2,1,0:T(8,128)S(1)} %fusion.95, pred[256,2048]{0,1:T(8,128)(4,1)S(1)} %broadcast_compare_fusion.2), kind=kOutput, calls=%fused_computation.105.clone.1 | convolution fusion | flops 276823040 | bytes 17698820 | tf_op jit(solution)/shard_map/cond/branch_1_fun/while/body/eval_jaxpr/qhr,kr->hqk/dot_general | solution.py:97
  85.2 2.1 convolution_convert_fusion.6
  87.4 6.0 %fusion.100 = f32[256,4,128]{0,2,1:T(8,128)} fusion(bf16[2048,4,128]{0,2,1:T(8,128)(2,1)S(1)} %bitcast.115, f32[4,256,2048]{1,2,0:T(8,128)} %get-tuple-element.497, f32[4,256]{1,0:T(4,128)S(1)} %get-tuple-element.528, pred[256,2048]{0,1:T(8,128)(4,1)S(1)} %broadcast_compare_fusion.2, f32[256,4,128]{0,2,1:T(8,128)} %get-tuple-element.516, ...), kind=kOutput, calls=%fused_computation.15.clone.1 | convolution fusion | flops 543555584 | bytes 12066817 | tf_op jit(solution)/shard_map/cond/branch_1_fun/while/body/eval_jaxpr/hqk,khv->qhv/dot_general | solution.py:107
  93.4 1.5 fusion.98
  95.5 2.0 convolution_convert_fusion.5
  97.6 1.3 fusion.95
  100.6 5.5 %fusion.96 = (f32[4,256]{1,0:T(4,128)S(1)}, f32[4,256,2048]{1,2,0:T(8,128)}) fusion(bf16[256,4,64]{0,2,1:T(8,128)(2,1)S(1)} %get-tuple-element.537, bf16[2,2048,64]{1,2,0:T(8,128)(2,1)S(1)} %get-tuple-element.536, s32[]{:T(128)} %get-tuple-element.513, f32[4,2048,256]{2,1,0:T(8,128)S(1)} %fusion.95, pred[256,2048]{0,1:T(8,128)(4,1)S(1)} %broadcast_compare_fusion.2), kind=kOutput, calls=%fused_computation.105.clone.1 | convolution fusion | flops 276823040 | bytes 17698820 | tf_op jit(solution)/shard_map/cond/branch_1_fun/while/body/eval_jaxpr/qhr,kr->hqk/dot_general | solution.py:97
  106.2 2.1 convolution_convert_fusion.6
  108.3 6.1 %fusion.100 = f32[256,4,128]{0,2,1:T(8,128)} fusion(bf16[2048,4,128]{0,2,1:T(8,128)(2,1)S(1)} %bitcast.115, f32[4,256,2048]{1,2,0:T(8,128)} %get-tuple-element.497, f32[4,256]{1,0:T(4,128)S(1)} %get-tuple-element.528, pred[256,2048]{0,1:T(8,128)(4,1)S(1)} %broadcast_compare_fusion.2, f32[256,4,128]{0,2,1:T(8,128)} %get-tuple-element.516, ...), kind=kOutput, calls=%fused_computation.15.clone.1 | convolution fusion | flops 543555584 | bytes 12066817 | tf_op jit(solution)/shard_map/cond/branch_1_fun/while/body/eval_jaxpr/hqk,khv->qhv/dot_general | solution.py:107
  114.4 1.5 fusion.98
  115.9 1.3 fusion.99
  118.5 3.9 %all_to_all.29 = bf16[2,128,512]{2,1,0:T(8,128)(2,1)S(1)} all-to-all(bf16[2,128,512]{2,1,0:T(8,128)(2,1)S(1)} %copy.65), channel_id=1, replica_groups=mesh['sp'=16,'tp'=2] {'tp'}, dimensions={0} | all-to-all | bytes 524288 | tf_op jit(solution)/shard_map/all_to_all | solution.py:138
  122.7 3.1 %multiply_reduce_fusion.1 = (f32[128]{0:T(128)S(1)}, f32[128,2048]{1,0:T(8,128)S(1)}) fusion(bf16[128,1024]{0,1:T(8,128)(2,1)S(1)} %bitcast.120, bf16[1024,2048]{1,0:T(8,128)(2,1)} %param.25, bf16[128,2048]{1,0:T(8,128)(2,1)} %param.18), kind=kOutput, calls=%fused_computation.66 | convolution fusion | flops 538443648 | bytes 6029824 | tf_op jit(solution)/shard_map/dot_general | solution.py:139
  128.9 3.5 %scatter_custom_fusion = bf16[512,2048]{1,0:T(8,128)(2,1)S(1)} fusion(s32[256]{0:T(256)S(1)} %bitcast.123, bf16[256,2048]{1,0:T(8,128)(2,1)} %reshape.245, bf16[]{:T(256)} %constant.158.clone.1), kind=kCustom, calls=%fused_computation.67 | custom fusion | bytes 2097664 | tf_op jit(solution)/shard_map/scatter | solution.py:160
  132.4 52.8 %all_to_all.30 = bf16[16,32,2048]{2,1,0:T(8,128)(2,1)} all-to-all(bf16[16,32,2048]{2,1,0:T(8,128)(2,1)S(1)} %bitcast.116), channel_id=1, replica_groups=mesh['sp'=16,'tp'=2] {'sp'}, dimensions={0} | all-to-all | bytes 4194304 | tf_op jit(solution)/shard_map/all_to_all | solution.py:166
  185.2 13.1 %all-gather.5.cloned.1.call-done = bf16[32,32,2048]{2,1,0:T(8,128)(2,1)} async-done(((bf16[16,32,2048]{2,1,0:T(8,128)(2,1)}), bf16[32,32,2048]{2,1,0:T(8,128)(2,1)}) %all-gather.5.cloned.1.call-update) | async-done | bytes 4194320 | tf_op jit(solution)/shard_map/all_gather | solution.py:165
  198.3 3.7 %fusion.36 = f32[32,32,256]{2,1,0:T(8,128)S(1)} fusion(bf16[32,32,2048]{2,1,0:T(8,128)(2,1)} %all-gather.5.cloned.1.call-done, bf16[1,2048,256]{2,1,0:T(8,128)(2,1)} %param.29), kind=kOutput, calls=%fused_computation.57 | convolution fusion | flops 1073741824 | bytes 6291456 | tf_op jit(solution)/shard_map/dot_general | solution.py:177
  202.1 8.5 %convolution_convert_fusion.2 = bf16[32,32,2048]{2,1,0:T(8,128)(2,1)} fusion(bf16[32,32,2048]{2,1,0:T(8,128)(2,1)} %all-gather.5.cloned.1.call-done, bf16[1,256,2048]{2,1,0:T(8,128)(2,1)S(1)} %copy-done, bf16[1,2048,256]{2,1,0:T(8,128)(2,1)S(1)} %copy-done.6, f32[32,32,256]{2,1,0:T(8,128)S(1)} %fusion.36), kind=kOutput, calls=%fused_computation.48 | convolution fusion | flops 2151153664 | bytes 11534336 | tf_op jit(solution)/shard_map/dot_general | solution.py:180
  210.6 13.5 %reduce-scatter.2.cloned.1.call-done = bf16[16,32,2048]{2,1,0:T(8,128)(2,1)} async-done(((bf16[32,32,2048]{2,1,0:T(8,128)(2,1)}), bf16[16,32,2048]{2,1,0:T(8,128)(2,1)}) %reduce-scatter.2.cloned.1.call-update) | async-done | bytes 2097168 | tf_op jit(solution)/shard_map/reduce_scatter | solution.py:181
  224.1 7.0 %all-to-all-start.2 = ((bf16[16,32,2048]{2,1,0:T(8,128)(2,1)}), bf16[16,32,2048]{2,1,0:T(8,128)(2,1)S(1)}, u32[]{:S(2)}, u32[]{:S(2)}) async-start(bf16[16,32,2048]{2,1,0:T(8,128)(2,1)} %reduce-scatter.2.cloned.1.call-done), calls=%async_computation.3 | async-start | bytes 4194304 | tf_op jit(solution)/shard_map/all_to_all | solution.py:189
  231.2 48.3 %all-to-all-done.2 = bf16[16,32,2048]{2,1,0:T(8,128)(2,1)S(1)} async-done(((bf16[16,32,2048]{2,1,0:T(8,128)(2,1)}), bf16[16,32,2048]{2,1,0:T(8,128)(2,1)S(1)}, u32[]{:S(2)}, u32[]{:S(2)}) %all-to-all-start.2) | async-done | bytes 2097184 | tf_op jit(solution)/shard_map/all_to_all | solution.py:189
  279.4 2.4 gather_fusion
  281.8 3.5 %reshape.232 = f32[128,2,2048]{2,1,0:T(2,128)} reshape(bf16[256,2048]{1,0:T(8,128)(2,1)} %gather_fusion) | data formatting | bytes 3145728 | tf_op jit(solution)/shard_map/convert_element_type | solution.py:192
  285.3 4.8 %multiply_reduce_fusion = f32[128,2048]{1,0:T(8,128)S(1)} fusion(f32[128,2,2048]{2,1,0:T(2,128)} %reshape.232, f32[128,2]{1,0:T(8,128)S(1)} %copy.62), kind=kLoop, calls=%fused_computation.52 | loop fusion | flops 786432 | bytes 3146752 | tf_op jit(solution)/shard_map/reduce_sum | solution.py:191
  (87 shorter events, 16.3 us)
Async XLA Ops:
  6.5 195.5 %copy-start = (bf16[1,256,2048]{2,1,0:T(8,128)(2,1)S(1)}, bf16[1,256,2048]{2,1,0:T(8,128)(2,1)}, u32[]{:S(2)}) copy-start(bf16[1,256,2048]{2,1,0:T(8,128)(2,1)} %param.31) | copy-start | bytes 3145732
  6.5 66.7 %all-gather.3.cloned.1.call-start = ((), (), s32[]{:S(2)}) async-start(), calls=%async_computation.4 | async-start | bytes 2228224 | tf_op jit(solution)/shard_map/all_gather | solution.py:74
  10.0 188.3 %all-gather.5.cloned.1.call-start = ((), (), s32[]{:S(2)}) async-start(), calls=%async_computation.5 | async-start | bytes 6291456 | tf_op jit(solution)/shard_map/all_gather | solution.py:165
  79.7 5.5 %copy-start.3 = (bf16[256,512]{1,0:T(8,128)(2,1)S(1)}, bf16[256,512]{1,0:T(8,128)(2,1)}, u32[]{:S(2)}) copy-start(bf16[256,512]{1,0:T(8,128)(2,1)} %get-tuple-element.538) | copy-start | bytes 786436 | tf_op jit(solution)/shard_map/cond/branch_1_fun/while
  85.2 8.2 %slice-start = ((s8[8388608]{0:T(1024)(128)(4,1)}), s8[4194304]{0:T(1024)(128)(4,1)S(1)}, s32[]{:S(2)}) async-start(s8[8388608]{0:T(1024)(128)(4,1)} %bitcast.110), calls=%async_computation.7 | async-start | bytes 8388608 | tf_op jit(solution)/shard_map/cond/branch_1_fun/while
  87.4 6.0 %slice-start.1 = ((s8[8388608]{0:T(1024)(128)(4,1)}), s8[4194304]{0:T(1024)(128)(4,1)S(1)}, s32[]{:S(2)}) async-start(s8[8388608]{0:T(1024)(128)(4,1)} %bitcast.110), calls=%async_computation.8 | async-start | bytes 8388608 | tf_op jit(solution)/shard_map/cond/branch_1_fun/while
  100.6 5.5 %copy-start.3 = (bf16[256,512]{1,0:T(8,128)(2,1)S(1)}, bf16[256,512]{1,0:T(8,128)(2,1)}, u32[]{:S(2)}) copy-start(bf16[256,512]{1,0:T(8,128)(2,1)} %get-tuple-element.538) | copy-start | bytes 786436 | tf_op jit(solution)/shard_map/cond/branch_1_fun/while
  106.2 8.2 %slice-start = ((s8[8388608]{0:T(1024)(128)(4,1)}), s8[4194304]{0:T(1024)(128)(4,1)S(1)}, s32[]{:S(2)}) async-start(s8[8388608]{0:T(1024)(128)(4,1)} %bitcast.110), calls=%async_computation.7 | async-start | bytes 8388608 | tf_op jit(solution)/shard_map/cond/branch_1_fun/while
  108.3 6.1 %slice-start.1 = ((s8[8388608]{0:T(1024)(128)(4,1)}), s8[4194304]{0:T(1024)(128)(4,1)S(1)}, s32[]{:S(2)}) async-start(s8[8388608]{0:T(1024)(128)(4,1)} %bitcast.110), calls=%async_computation.8 | async-start | bytes 8388608 | tf_op jit(solution)/shard_map/cond/branch_1_fun/while
  118.3 8.6 %copy-start.4 = (f32[2048]{0:T(1024)S(1)}, f32[2048]{0:T(1024)}, u32[]{:S(2)}) copy-start(f32[2048]{0:T(1024)} %param.26) | copy-start | bytes 24580
  125.8 1.1 copy-start.1
  185.2 16.9 %copy-start.6 = (bf16[1,2048,256]{2,1,0:T(8,128)(2,1)S(1)}, bf16[1,2048,256]{2,1,0:T(8,128)(2,1)}, u32[]{:S(2)}) copy-start(bf16[1,2048,256]{2,1,0:T(8,128)(2,1)} %param.30) | copy-start | bytes 3145732
  185.2 38.9 %reduce-scatter.2.cloned.1.call-start = ((), (), s32[]{:S(2)}) async-start(), calls=%async_computation.6 | async-start | bytes 6291456 | tf_op jit(solution)/shard_map/reduce_scatter | solution.py:181
  210.6 20.5 %copy-start.5 = (f32[128,2]{0,1:T(2,128)S(1)}, f32[128,2]{0,1:T(2,128)}, u32[]{:S(2)}) copy-start(f32[128,2]{0,1:T(2,128)} %param.28) | copy-start | bytes 3076
  224.1 55.4 %all-to-all-start.2 = ((bf16[16,32,2048]{2,1,0:T(8,128)(2,1)}), bf16[16,32,2048]{2,1,0:T(8,128)(2,1)S(1)}, u32[]{:S(2)}, u32[]{:S(2)}) async-start(bf16[16,32,2048]{2,1,0:T(8,128)(2,1)} %reduce-scatter.2.cloned.1.call-done), calls=%async_computation.3 | async-start | bytes 4194304 | tf_op jit(solution)/shard_map/all_to_all | solution.py:189
  281.8 8.3 %copy-start.2 = (f32[128,2048]{1,0:T(8,128)S(1)}, f32[128,2048]{1,0:T(8,128)}, u32[]{:S(2)}) copy-start(f32[128,2048]{1,0:T(8,128)} %copy-done.1) | copy-start | bytes 3145732
Sparse Core Ops, SparseCore 0:
  10.2 63.0 all-gather.2
  185.3 12.9 all-gather.4
  210.7 13.2 reduce-scatter.1
where the time goes:
time: 298 us
  blocking collectives  97.9 us (33%)
  waiting for transfers between devices  95.1 us (32%)
  matrix products  49.3 us (17%)
  local copies, waits for them, and re-layouts  17.9 us (6%)
  other arithmetic  16.7 us (6%)
  between operations  13.3 us (4%)
  starting transfers between devices  7.08 us (2%)
    all_to_all x1, blocking collectives, local(): lax.all_to_all(outgoing.reshape(expert_count, capacity, width), 'sp', spl...  52.8 us
    all_to_all x1, waiting for transfers between devices, local(): lax.all_to_all(summed, 'sp', split_axis=0, concat_axis=0, tiled=True)  48.3 us
    all_gather x1, blocking collectives, local(): rot_rows = lax.all_gather(paired[1], 'sp', axis=0, tiled=True)  35.9 us
    all_gather x1, waiting for transfers between devices, local(): lat_rows = lax.all_gather(paired[0], 'sp', axis=0, tiled=True)  20.2 us
    reduce_scatter x1, waiting for transfers between devices, local(): lax.psum_scatter(lax.optimization_barrier(product.astype(jnp.bfloat16)).a...  13.5 us
    all_gather x1, waiting for transfers between devices, local(): lax.all_gather(lax.all_to_all(outgoing.reshape(expert_count, capacity, wi...  13.1 us
    dot_general x2, matrix products, one_block(): jnp.einsum('hqk,khv->qhv', weights.astype(jnp.bfloat16), value_rows, pref...  12.1 us
    dot_general x2, matrix products, one_block(): jnp.einsum('qhr,kr->hqk', query_rot, rot_block, preferred_element_type=jn...  11 us
  transfers between devices with their start and end apart: 4, of which 4 were waited for; matrix products, arithmetic and copies ran while one was open for 2% of the time, Pallas kernels for 0%

commit v1 on v0

--- a/solution.py
+++ b/solution.py
@@ -72,7 +72,12 @@
         lax.all_gather(key_rot, "tp", axis=0, tiled=True),
     )
     lat_rows = lax.all_gather(paired[0], "sp", axis=0, tiled=True)
-    rot_rows = lax.all_gather(paired[1], "sp", axis=0, tiled=True)
+    ring = [paired[1]]
+    for hop in range(15):
+        ring.append(lax.ppermute(ring[-1], "sp", [(dev, (dev + 1) % 16) for dev in range(16)]))
+    rot_rows = jnp.roll(
+        jnp.concatenate(ring[::-1], axis=0), (lax.axis_index("sp") + 1) * ring[0].shape[0], axis=0
+    )
     piece_rows = lat_rows.shape[0]
     key_block = piece_rows
     while key_block > 2048 and key_block % 2 == 0:

time: 298 us -> 368 us (1.23)
  starting transfers between devices: 7.08 us -> 52.6 us
  local copies, waits for them, and re-layouts: 17.9 us -> 37.9 us
  waiting for transfers between devices: 95.1 us -> 110 us
  blocking collectives: 97.9 us -> 86.8 us
    ppermute x0 -> x15, starting transfers between devices: none -> 45.5 us  [local(): lax.ppermute(ring[-1], 'sp', [(dev, (dev + 1) % 16) for dev in range(16)])]
    all_gather x1 -> x0, blocking collectives: 35.9 us -> none  [local(): rot_rows = lax.all_gather(paired[1], 'sp', axis=0, tiled=True)]
    ppermute x0 -> x15, waiting for transfers between devices: none -> 35.2 us  [local(): lax.ppermute(ring[-1], 'sp', [(dev, (dev + 1) % 16) for dev in range(16)])]
    all_to_all x1, blocking collectives: 52.8 us -> 77.7 us  [local(): lax.all_to_all(outgoing.reshape(expert_count, capacity, width), 'sp', spl...]
    all_gather x1, waiting for transfers between devices: 20.2 us -> 0.01 us  [local(): lat_rows = lax.all_gather(paired[0], 'sp', axis=0, tiled=True)]
    unnamed x14 -> x53, local copies, waits for them, and re-layouts: 1.96 us -> 21.1 us
  transfers between devices with their start and end apart: 4 -> 19, of which waited for: 4 -> 17; matrix products, arithmetic and copies ran while one was open for 2% -> 7% of each run, Pallas kernels for 0% -> 0%
where the time goes in v1:
time: 368 us; the launch traced here: 367 us
  waiting for transfers between devices  110 us (30%)
  blocking collectives  86.8 us (24%)
  starting transfers between devices  52.6 us (14%)
  matrix products  49.2 us (13%)
  local copies, waits for them, and re-layouts  37.9 us (10%)
  other arithmetic  16.8 us (5%)
  between operations  13.4 us (4%)
    all_to_all x1, blocking collectives, local(): lax.all_to_all(outgoing.reshape(expert_count, capacity, width), 'sp', spl...  77.7 us
    all_to_all x1, waiting for transfers between devices, local(): lax.all_to_all(summed, 'sp', split_axis=0, concat_axis=0, tiled=True)  48.2 us
    ppermute x15, starting transfers between devices, local(): lax.ppermute(ring[-1], 'sp', [(dev, (dev + 1) % 16) for dev in range(16)])  45.5 us
    ppermute x15, waiting for transfers between devices, local(): lax.ppermute(ring[-1], 'sp', [(dev, (dev + 1) % 16) for dev in range(16)])  35.2 us
    unnamed x53, local copies, waits for them, and re-layouts  21.1 us
    reduce_scatter x1, waiting for transfers between devices, local(): lax.psum_scatter(lax.optimization_barrier(product.astype(jnp.bfloat16)).a...  13.5 us
    all_gather x1, waiting for transfers between devices, local(): lax.all_gather(lax.all_to_all(outgoing.reshape(expert_count, capacity, wi...  13 us
    dot_general x2, matrix products, one_block(): jnp.einsum('hqk,khv->qhv', weights.astype(jnp.bfloat16), value_rows, pref...  12.1 us
  transfers between devices with their start and end apart: 19, of which 17 were waited for; matrix products, arithmetic and copies ran while one was open for 7% of the time, Pallas kernels for 0%

profile of v1, /device:TPU:12, one launch (start us, length us, event | category | flops | bytes accessed | tf_op | source)
XLA Modules:
  0.0 366.9 jit_solution(14718583798354669532)
XLA Ops:
  11.0 3.3 collective-permute-done
  14.9 4.2 %collective-permute-done.1 = bf16[256,64]{0,1:T(8,128)(2,1)S(1)} collective-permute-done((bf16[256,64]{0,1:T(8,128)(2,1)S(1)}, bf16[256,64]{0,1:T(8,128)(2,1)S(1)}, u32[]{:S(2)}, u32[]{:S(2)}) %collective-permute-start.1) | collective-permute-done | bytes 32800 | tf_op jit(solution)/shard_map/ppermute | solution.py:77
  19.8 4.1 %collective-permute-done.2 = bf16[256,64]{0,1:T(8,128)(2,1)S(1)} collective-permute-done((bf16[256,64]{0,1:T(8,128)(2,1)S(1)}, bf16[256,64]{0,1:T(8,128)(2,1)S(1)}, u32[]{:S(2)}, u32[]{:S(2)}) %collective-permute-start.2) | collective-permute-done | bytes 32800 | tf_op jit(solution)/shard_map/ppermute | solution.py:77
  25.5 3.3 all_gather.12
  28.9 4.2 %collective-permute-start.4 = (bf16[256,64]{0,1:T(8,128)(2,1)S(1)}, bf16[256,64]{0,1:T(8,128)(2,1)S(1)}, u32[]{:S(2)}, u32[]{:S(2)}) collective-permute-start(bf16[256,64]{0,1:T(8,128)(2,1)S(1)} %collective-permute-done.3), channel_id=1, source_target_pairs={{0,2},{2,4},{4,6},{6,8},{8,10},{10,12},{12,14},{14,16},{16,18},{18... | collective-permute-start | bytes 98312 | tf_op jit(solution)/shard_map/ppermute | solution.py:77
  39.5 3.1 collective-permute-start.6
  44.4 4.7 %collective-permute-start.7 = (bf16[256,64]{0,1:T(8,128)(2,1)S(1)}, bf16[256,64]{0,1:T(8,128)(2,1)S(1)}, u32[]{:S(2)}, u32[]{:S(2)}) collective-permute-start(bf16[256,64]{0,1:T(8,128)(2,1)S(1)} %collective-permute-done.6), channel_id=1, source_target_pairs={{0,2},{2,4},{4,6},{6,8},{8,10},{10,12},{12,14},{14,16},{16,18},{18... | collective-permute-start | bytes 98312 | tf_op jit(solution)/shard_map/ppermute | solution.py:77
  50.8 4.3 %collective-permute-start.8 = (bf16[256,64]{0,1:T(8,128)(2,1)S(1)}, bf16[256,64]{0,1:T(8,128)(2,1)S(1)}, u32[]{:S(2)}, u32[]{:S(2)}) collective-permute-start(bf16[256,64]{0,1:T(8,128)(2,1)S(1)} %collective-permute-done.7), channel_id=1, source_target_pairs={{0,2},{2,4},{4,6},{6,8},{8,10},{10,12},{12,14},{14,16},{16,18},{18... | collective-permute-start | bytes 98312 | tf_op jit(solution)/shard_map/ppermute | solution.py:77
  56.6 4.1 %collective-permute-start.9 = (bf16[256,64]{0,1:T(8,128)(2,1)S(1)}, bf16[256,64]{0,1:T(8,128)(2,1)S(1)}, u32[]{:S(2)}, u32[]{:S(2)}) collective-permute-start(bf16[256,64]{0,1:T(8,128)(2,1)S(1)} %collective-permute-done.8), channel_id=1, source_target_pairs={{0,2},{2,4},{4,6},{6,8},{8,10},{10,12},{12,14},{14,16},{16,18},{18... | collective-permute-start | bytes 98312 | tf_op jit(solution)/shard_map/ppermute | solution.py:77
  62.4 4.1 %collective-permute-start.10 = (bf16[256,64]{0,1:T(8,128)(2,1)S(1)}, bf16[256,64]{0,1:T(8,128)(2,1)S(1)}, u32[]{:S(2)}, u32[]{:S(2)}) collective-permute-start(bf16[256,64]{0,1:T(8,128)(2,1)S(1)} %collective-permute-done.9), channel_id=1, source_target_pairs={{0,2},{2,4},{4,6},{6,8},{8,10},{10,12},{12,14},{14,16},{16,18},{18... | collective-permute-start | bytes 98312 | tf_op jit(solution)/shard_map/ppermute | solution.py:77
  68.4 4.0 %collective-permute-start.11 = (bf16[256,64]{0,1:T(8,128)(2,1)S(1)}, bf16[256,64]{0,1:T(8,128)(2,1)S(1)}, u32[]{:S(2)}, u32[]{:S(2)}) collective-permute-start(bf16[256,64]{0,1:T(8,128)(2,1)S(1)} %collective-permute-done.10), channel_id=1, source_target_pairs={{0,2},{2,4},{4,6},{6,8},{8,10},{10,12},{12,14},{14,16},{16,18},{18... | collective-permute-start | bytes 98312 | tf_op jit(solution)/shard_map/ppermute | solution.py:77
  74.0 4.6 %collective-permute-start.12 = (bf16[256,64]{0,1:T(8,128)(2,1)S(1)}, bf16[256,64]{0,1:T(8,128)(2,1)S(1)}, u32[]{:S(2)}, u32[]{:S(2)}) collective-permute-start(bf16[256,64]{0,1:T(8,128)(2,1)S(1)} %collective-permute-done.11), channel_id=1, source_target_pairs={{0,2},{2,4},{4,6},{6,8},{8,10},{10,12},{12,14},{14,16},{16,18},{18... | collective-permute-start | bytes 98312 | tf_op jit(solution)/shard_map/ppermute | solution.py:77
  81.4 4.3 %collective-permute-start.13 = (bf16[256,64]{0,1:T(8,128)(2,1)S(1)}, bf16[256,64]{0,1:T(8,128)(2,1)S(1)}, u32[]{:S(2)}, u32[]{:S(2)}) collective-permute-start(bf16[256,64]{0,1:T(8,128)(2,1)S(1)} %collective-permute-done.12), channel_id=1, source_target_pairs={{0,2},{2,4},{4,6},{6,8},{8,10},{10,12},{12,14},{14,16},{16,18},{18... | collective-permute-start | bytes 98312 | tf_op jit(solution)/shard_map/ppermute | solution.py:77
  85.7 4.6 %collective-permute-done.13 = bf16[256,64]{0,1:T(8,128)(2,1)S(1)} collective-permute-done((bf16[256,64]{0,1:T(8,128)(2,1)S(1)}, bf16[256,64]{0,1:T(8,128)(2,1)S(1)}, u32[]{:S(2)}, u32[]{:S(2)}) %collective-permute-start.13) | collective-permute-done | bytes 32800 | tf_op jit(solution)/shard_map/ppermute | solution.py:77
  91.8 6.0 %collective-permute-done.14 = bf16[256,64]{0,1:T(8,128)(2,1)S(1)} collective-permute-done((bf16[256,64]{0,1:T(8,128)(2,1)S(1)}, bf16[256,64]{0,1:T(8,128)(2,1)S(1)}, u32[]{:S(2)}, u32[]{:S(2)}) %collective-permute-start.14) | collective-permute-done | bytes 32800 | tf_op jit(solution)/shard_map/ppermute | solution.py:77
  117.6 44.2 %conditional.1 = (f32[4,256]{1,0:T(4,128)}, f32[256,4,128]{0,2,1:T(8,128)}) conditional(s32[]{:T(128)} %convert_element_type.80, () %tuple.45, (bf16[4096,256]{1,0:T(8,128)(2,1)}, s32[]{:T(128)}, s32[]{:T(128)}, bf16[8192,64]{0,1:T(8,128)(2,1)}, bf16[256,512]{1,0:T(8,128)(2,1)S(1)}, /*index=5*/s32[256]{0:T(256)S(1)}, s32[256]{0:T(256)S(1)}, ...), branch_computations={%region_0.1_spmd, %region_1.6_spmd.clone} | conditional | flops 2439948032 | bytes 85153400 | solution.py:135
  119.3 42.5 %while.26 = (s32[]{:T(128)}, f32[4,256]{1,0:T(4,128)S(1)}, f32[4,256]{1,0:T(4,128)}, f32[256,4,128]{0,2,1:T(8,128)}, s32[2]{0:T(128)S(1)}, /*index=5*/s32[256]{0...) while((s32[]{:T(128)}, f32[4,256]{1,0:T(4,128)S(1)}, ...), condition=%wide.region_5.5_spmd.clone, body=%wide.region_2.4_spmd.clone.sunk | while | flops 2439944192 | bytes 82004296 | solution.py:121
  124.4 5.5 %fusion.96 = (f32[4,256]{1,0:T(4,128)S(1)}, f32[4,256,2048]{1,2,0:T(8,128)}) fusion(bf16[256,4,64]{0,2,1:T(8,128)(2,1)S(1)} %get-tuple-element.690, bf16[2,2048,64]{1,2,0:T(8,128)(2,1)S(1)} %get-tuple-element.689, s32[]{:T(128)} %get-tuple-element.666, f32[4,2048,256]{2,1,0:T(8,128)S(1)} %fusion.95, pred[256,2048]{0,1:T(8,128)(4,1)S(1)} %broadcast_compare_fusion.2), kind=kOutput, calls=%fused_computation.138.clone.1 | convolution fusion | flops 276823040 | bytes 17698820 | tf_op jit(solution)/shard_map/cond/branch_1_fun/while/body/eval_jaxpr/qhr,kr->hqk/dot_general | solution.py:102
  132.1 6.0 %fusion.100 = f32[256,4,128]{0,2,1:T(8,128)} fusion(bf16[2048,4,128]{0,2,1:T(8,128)(2,1)S(1)} %bitcast.115, f32[4,256,2048]{1,2,0:T(8,128)} %get-tuple-element.650, f32[4,256]{1,0:T(4,128)S(1)} %get-tuple-element.681, pred[256,2048]{0,1:T(8,128)(4,1)S(1)} %broadcast_compare_fusion.2, f32[256,4,128]{0,2,1:T(8,128)} %get-tuple-element.669, ...), kind=kOutput, calls=%fused_computation.15.clone.1 | convolution fusion | flops 543555584 | bytes 12066817 | tf_op jit(solution)/shard_map/cond/branch_1_fun/while/body/eval_jaxpr/hqk,khv->qhv/dot_general | solution.py:112
  145.3 5.5 %fusion.96 = (f32[4,256]{1,0:T(4,128)S(1)}, f32[4,256,2048]{1,2,0:T(8,128)}) fusion(bf16[256,4,64]{0,2,1:T(8,128)(2,1)S(1)} %get-tuple-element.690, bf16[2,2048,64]{1,2,0:T(8,128)(2,1)S(1)} %get-tuple-element.689, s32[]{:T(128)} %get-tuple-element.666, f32[4,2048,256]{2,1,0:T(8,128)S(1)} %fusion.95, pred[256,2048]{0,1:T(8,128)(4,1)S(1)} %broadcast_compare_fusion.2), kind=kOutput, calls=%fused_computation.138.clone.1 | convolution fusion | flops 276823040 | bytes 17698820 | tf_op jit(solution)/shard_map/cond/branch_1_fun/while/body/eval_jaxpr/qhr,kr->hqk/dot_general | solution.py:102
  153.0 6.1 %fusion.100 = f32[256,4,128]{0,2,1:T(8,128)} fusion(bf16[2048,4,128]{0,2,1:T(8,128)(2,1)S(1)} %bitcast.115, f32[4,256,2048]{1,2,0:T(8,128)} %get-tuple-element.650, f32[4,256]{1,0:T(4,128)S(1)} %get-tuple-element.681, pred[256,2048]{0,1:T(8,128)(4,1)S(1)} %broadcast_compare_fusion.2, f32[256,4,128]{0,2,1:T(8,128)} %get-tuple-element.669, ...), kind=kOutput, calls=%fused_computation.15.clone.1 | convolution fusion | flops 543555584 | bytes 12066817 | tf_op jit(solution)/shard_map/cond/branch_1_fun/while/body/eval_jaxpr/hqk,khv->qhv/dot_general | solution.py:112
  163.2 3.9 %all_to_all.29 = bf16[2,128,512]{2,1,0:T(8,128)(2,1)S(1)} all-to-all(bf16[2,128,512]{2,1,0:T(8,128)(2,1)S(1)} %copy.65), channel_id=1, replica_groups=mesh['sp'=16,'tp'=2] {'tp'}, dimensions={0} | all-to-all | bytes 524288 | tf_op jit(solution)/shard_map/all_to_all | solution.py:143
  173.4 3.5 scatter_custom_fusion
  176.9 77.7 %all_to_all.30 = bf16[16,32,2048]{2,1,0:T(8,128)(2,1)} all-to-all(bf16[16,32,2048]{2,1,0:T(8,128)(2,1)S(1)} %bitcast.116), channel_id=1, replica_groups=mesh['sp'=16,'tp'=2] {'sp'}, dimensions={0} | all-to-all | bytes 4194304 | tf_op jit(solution)/shard_map/all_to_all | solution.py:171
  254.6 13.0 %all-gather.5.cloned.1.call-done = bf16[32,32,2048]{2,1,0:T(8,128)(2,1)} async-done(((bf16[16,32,2048]{2,1,0:T(8,128)(2,1)}), bf16[32,32,2048]{2,1,0:T(8,128)(2,1)}) %all-gather.5.cloned.1.call-update) | async-done | bytes 4194320 | tf_op jit(solution)/shard_map/all_gather | solution.py:170
  267.7 3.7 %fusion.36 = f32[32,32,256]{2,1,0:T(8,128)S(1)} fusion(bf16[32,32,2048]{2,1,0:T(8,128)(2,1)} %all-gather.5.cloned.1.call-done, bf16[1,2048,256]{2,1,0:T(8,128)(2,1)} %param.29), kind=kOutput, calls=%fused_computation.58 | convolution fusion | flops 1073741824 | bytes 6291456 | tf_op jit(solution)/shard_map/dot_general | solution.py:182
  271.4 8.5 %convolution_convert_fusion.2 = bf16[32,32,2048]{2,1,0:T(8,128)(2,1)} fusion(bf16[32,32,2048]{2,1,0:T(8,128)(2,1)} %all-gather.5.cloned.1.call-done, bf16[1,256,2048]{2,1,0:T(8,128)(2,1)S(1)} %copy-done, bf16[1,2048,256]{2,1,0:T(8,128)(2,1)S(1)} %copy-done.9, f32[32,32,256]{2,1,0:T(8,128)S(1)} %fusion.36), kind=kOutput, calls=%fused_computation.49 | convolution fusion | flops 2151153664 | bytes 11534336 | tf_op jit(solution)/shard_map/dot_general | solution.py:185
  280.0 13.5 %reduce-scatter.2.cloned.1.call-done = bf16[16,32,2048]{2,1,0:T(8,128)(2,1)} async-done(((bf16[32,32,2048]{2,1,0:T(8,128)(2,1)}), bf16[16,32,2048]{2,1,0:T(8,128)(2,1)}) %reduce-scatter.2.cloned.1.call-update) | async-done | bytes 2097168 | tf_op jit(solution)/shard_map/reduce_scatter | solution.py:186
  293.5 7.0 %all-to-all-start.2 = ((bf16[16,32,2048]{2,1,0:T(8,128)(2,1)}), bf16[16,32,2048]{2,1,0:T(8,128)(2,1)S(1)}, u32[]{:S(2)}, u32[]{:S(2)}) async-start(bf16[16,32,2048]{2,1,0:T(8,128)(2,1)} %reduce-scatter.2.cloned.1.call-done), calls=%async_computation.3 | async-start | bytes 4194304 | tf_op jit(solution)/shard_map/all_to_all | solution.py:194
  300.6 48.2 %all-to-all-done.2 = bf16[16,32,2048]{2,1,0:T(8,128)(2,1)S(1)} async-done(((bf16[16,32,2048]{2,1,0:T(8,128)(2,1)}), bf16[16,32,2048]{2,1,0:T(8,128)(2,1)S(1)}, u32[]{:S(2)}, u32[]{:S(2)}) %all-to-all-start.2) | async-done | bytes 2097184 | tf_op jit(solution)/shard_map/all_to_all | solution.py:194
  351.2 3.4 reshape.238
  354.6 4.8 %multiply_reduce_fusion = f32[128,2048]{1,0:T(8,128)S(1)} fusion(f32[128,2,2048]{2,1,0:T(2,128)} %reshape.238, f32[128,2]{1,0:T(8,128)S(1)} %copy.62), kind=kLoop, calls=%fused_computation.53 | loop fusion | flops 786432 | bytes 3146752 | tf_op jit(solution)/shard_map/reduce_sum | solution.py:196
  (161 shorter events, 79.8 us)
Async XLA Ops:
  6.5 264.9 %copy-start = (bf16[1,256,2048]{2,1,0:T(8,128)(2,1)S(1)}, bf16[1,256,2048]{2,1,0:T(8,128)(2,1)}, u32[]{:S(2)}) copy-start(bf16[1,256,2048]{2,1,0:T(8,128)(2,1)} %param.31) | copy-start | bytes 3145732
  6.5 111.0 %copy-start.6 = (bf16[256,512]{1,0:T(8,128)(2,1)S(1)}, bf16[256,512]{1,0:T(8,128)(2,1)}, u32[]{:S(2)}) copy-start(bf16[256,512]{1,0:T(8,128)(2,1)} %param.19) | copy-start | bytes 786436
  6.5 111.0 %copy-start.3 = (bf16[256,512]{1,0:T(8,128)(2,1)S(1)}, bf16[256,512]{1,0:T(8,128)(2,1)}, u32[]{:S(2)}) copy-start(bf16[256,512]{1,0:T(8,128)(2,1)} %param.23) | copy-start | bytes 786436
  6.5 111.0 %copy-start.4 = (bf16[256,512]{1,0:T(8,128)(2,1)S(1)}, bf16[256,512]{1,0:T(8,128)(2,1)}, u32[]{:S(2)}) copy-start(bf16[256,512]{1,0:T(8,128)(2,1)} %param.24) | copy-start | bytes 786436
  6.5 111.0 %all-gather.3.cloned.1.call-start = ((), (), s32[]{:S(2)}) async-start(), calls=%async_computation.4 | async-start | bytes 2228224 | tf_op jit(solution)/shard_map/all_gather | solution.py:74
  9.5 4.8 %collective-permute-start = (bf16[256,64]{0,1:T(8,128)(2,1)S(1)}, bf16[256,64]{0,1:T(8,128)(2,1)S(1)}, u32[]{:S(2)}, u32[]{:S(2)}) collective-permute-start(bf16[256,64]{0,1:T(8,128)(2,1)S(1)} %all_gather.14), channel_id=1, source_target_pairs={{0,2},{2,4},{4,6},{6,8},{8,10},{10,12},{12,14},{14,16},{16,18},{18... | collective-permute-start | bytes 98312 | tf_op jit(solution)/shard_map/ppermute | solution.py:77
  14.3 4.8 %collective-permute-start.1 = (bf16[256,64]{0,1:T(8,128)(2,1)S(1)}, bf16[256,64]{0,1:T(8,128)(2,1)S(1)}, u32[]{:S(2)}, u32[]{:S(2)}) collective-permute-start(bf16[256,64]{0,1:T(8,128)(2,1)S(1)} %collective-permute-done), channel_id=1, source_target_pairs={{0,2},{2,4},{4,6},{6,8},{8,10},{10,12},{12,14},{14,16},{16,18},{18... | collective-permute-start | bytes 98312 | tf_op jit(solution)/shard_map/ppermute | solution.py:77
  19.1 4.8 %collective-permute-start.2 = (bf16[256,64]{0,1:T(8,128)(2,1)S(1)}, bf16[256,64]{0,1:T(8,128)(2,1)S(1)}, u32[]{:S(2)}, u32[]{:S(2)}) collective-permute-start(bf16[256,64]{0,1:T(8,128)(2,1)S(1)} %collective-permute-done.1), channel_id=1, source_target_pairs={{0,2},{2,4},{4,6},{6,8},{8,10},{10,12},{12,14},{14,16},{16,18},{18... | collective-permute-start | bytes 98312 | tf_op jit(solution)/shard_map/ppermute | solution.py:77
  23.9 5.0 %collective-permute-start.3 = (bf16[256,64]{0,1:T(8,128)(2,1)S(1)}, bf16[256,64]{0,1:T(8,128)(2,1)S(1)}, u32[]{:S(2)}, u32[]{:S(2)}) collective-permute-start(bf16[256,64]{0,1:T(8,128)(2,1)S(1)} %collective-permute-done.2), channel_id=1, source_target_pairs={{0,2},{2,4},{4,6},{6,8},{8,10},{10,12},{12,14},{14,16},{16,18},{18... | collective-permute-start | bytes 98312 | tf_op jit(solution)/shard_map/ppermute | solution.py:77
  28.9 238.8 %all-gather.5.cloned.1.call-start = ((), (), s32[]{:S(2)}) async-start(), calls=%async_computation.5 | async-start | bytes 6291456 | tf_op jit(solution)/shard_map/all_gather | solution.py:170
  28.9 5.8 %collective-permute-start.4 = (bf16[256,64]{0,1:T(8,128)(2,1)S(1)}, bf16[256,64]{0,1:T(8,128)(2,1)S(1)}, u32[]{:S(2)}, u32[]{:S(2)}) collective-permute-start(bf16[256,64]{0,1:T(8,128)(2,1)S(1)} %collective-permute-done.3), channel_id=1, source_target_pairs={{0,2},{2,4},{4,6},{6,8},{8,10},{10,12},{12,14},{14,16},{16,18},{18... | collective-permute-start | bytes 98312 | tf_op jit(solution)/shard_map/ppermute | solution.py:77
  34.7 4.8 %collective-permute-start.5 = (bf16[256,64]{0,1:T(8,128)(2,1)S(1)}, bf16[256,64]{0,1:T(8,128)(2,1)S(1)}, u32[]{:S(2)}, u32[]{:S(2)}) collective-permute-start(bf16[256,64]{0,1:T(8,128)(2,1)S(1)} %collective-permute-done.4), channel_id=1, source_target_pairs={{0,2},{2,4},{4,6},{6,8},{8,10},{10,12},{12,14},{14,16},{16,18},{18... | collective-permute-start | bytes 98312 | tf_op jit(solution)/shard_map/ppermute | solution.py:77
  39.5 4.9 %collective-permute-start.6 = (bf16[256,64]{0,1:T(8,128)(2,1)S(1)}, bf16[256,64]{0,1:T(8,128)(2,1)S(1)}, u32[]{:S(2)}, u32[]{:S(2)}) collective-permute-start(bf16[256,64]{0,1:T(8,128)(2,1)S(1)} %collective-permute-done.5), channel_id=1, source_target_pairs={{0,2},{2,4},{4,6},{6,8},{8,10},{10,12},{12,14},{14,16},{16,18},{18... | collective-permute-start | bytes 98312 | tf_op jit(solution)/shard_map/ppermute | solution.py:77
  44.4 6.3 %collective-permute-start.7 = (bf16[256,64]{0,1:T(8,128)(2,1)S(1)}, bf16[256,64]{0,1:T(8,128)(2,1)S(1)}, u32[]{:S(2)}, u32[]{:S(2)}) collective-permute-start(bf16[256,64]{0,1:T(8,128)(2,1)S(1)} %collective-permute-done.6), channel_id=1, source_target_pairs={{0,2},{2,4},{4,6},{6,8},{8,10},{10,12},{12,14},{14,16},{16,18},{18... | collective-permute-start | bytes 98312 | tf_op jit(solution)/shard_map/ppermute | solution.py:77
  50.8 5.9 %collective-permute-start.8 = (bf16[256,64]{0,1:T(8,128)(2,1)S(1)}, bf16[256,64]{0,1:T(8,128)(2,1)S(1)}, u32[]{:S(2)}, u32[]{:S(2)}) collective-permute-start(bf16[256,64]{0,1:T(8,128)(2,1)S(1)} %collective-permute-done.7), channel_id=1, source_target_pairs={{0,2},{2,4},{4,6},{6,8},{8,10},{10,12},{12,14},{14,16},{16,18},{18... | collective-permute-start | bytes 98312 | tf_op jit(solution)/shard_map/ppermute | solution.py:77
  56.6 5.7 %collective-permute-start.9 = (bf16[256,64]{0,1:T(8,128)(2,1)S(1)}, bf16[256,64]{0,1:T(8,128)(2,1)S(1)}, u32[]{:S(2)}, u32[]{:S(2)}) collective-permute-start(bf16[256,64]{0,1:T(8,128)(2,1)S(1)} %collective-permute-done.8), channel_id=1, source_target_pairs={{0,2},{2,4},{4,6},{6,8},{8,10},{10,12},{12,14},{14,16},{16,18},{18... | collective-permute-start | bytes 98312 | tf_op jit(solution)/shard_map/ppermute | solution.py:77
  62.4 6.0 %collective-permute-start.10 = (bf16[256,64]{0,1:T(8,128)(2,1)S(1)}, bf16[256,64]{0,1:T(8,128)(2,1)S(1)}, u32[]{:S(2)}, u32[]{:S(2)}) collective-permute-start(bf16[256,64]{0,1:T(8,128)(2,1)S(1)} %collective-permute-done.9), channel_id=1, source_target_pairs={{0,2},{2,4},{4,6},{6,8},{8,10},{10,12},{12,14},{14,16},{16,18},{18... | collective-permute-start | bytes 98312 | tf_op jit(solution)/shard_map/ppermute | solution.py:77
  68.4 5.6 %collective-permute-start.11 = (bf16[256,64]{0,1:T(8,128)(2,1)S(1)}, bf16[256,64]{0,1:T(8,128)(2,1)S(1)}, u32[]{:S(2)}, u32[]{:S(2)}) collective-permute-start(bf16[256,64]{0,1:T(8,128)(2,1)S(1)} %collective-permute-done.10), channel_id=1, source_target_pairs={{0,2},{2,4},{4,6},{6,8},{8,10},{10,12},{12,14},{14,16},{16,18},{18... | collective-permute-start | bytes 98312 | tf_op jit(solution)/shard_map/ppermute | solution.py:77
  74.0 7.4 %collective-permute-start.12 = (bf16[256,64]{0,1:T(8,128)(2,1)S(1)}, bf16[256,64]{0,1:T(8,128)(2,1)S(1)}, u32[]{:S(2)}, u32[]{:S(2)}) collective-permute-start(bf16[256,64]{0,1:T(8,128)(2,1)S(1)} %collective-permute-done.11), channel_id=1, source_target_pairs={{0,2},{2,4},{4,6},{6,8},{8,10},{10,12},{12,14},{14,16},{16,18},{18... | collective-permute-start | bytes 98312 | tf_op jit(solution)/shard_map/ppermute | solution.py:77
  81.4 8.9 %collective-permute-start.13 = (bf16[256,64]{0,1:T(8,128)(2,1)S(1)}, bf16[256,64]{0,1:T(8,128)(2,1)S(1)}, u32[]{:S(2)}, u32[]{:S(2)}) collective-permute-start(bf16[256,64]{0,1:T(8,128)(2,1)S(1)} %collective-permute-done.12), channel_id=1, source_target_pairs={{0,2},{2,4},{4,6},{6,8},{8,10},{10,12},{12,14},{14,16},{16,18},{18... | collective-permute-start | bytes 98312 | tf_op jit(solution)/shard_map/ppermute | solution.py:77
  90.3 7.5 %collective-permute-start.14 = (bf16[256,64]{0,1:T(8,128)(2,1)S(1)}, bf16[256,64]{0,1:T(8,128)(2,1)S(1)}, u32[]{:S(2)}, u32[]{:S(2)}) collective-permute-start(bf16[256,64]{0,1:T(8,128)(2,1)S(1)} %collective-permute-done.13), channel_id=1, source_target_pairs={{0,2},{2,4},{4,6},{6,8},{8,10},{10,12},{12,14},{14,16},{16,18},{18... | collective-permute-start | bytes 98312 | tf_op jit(solution)/shard_map/ppermute | solution.py:77
  117.6 49.7 %copy-start.5 = (bf16[128,2048]{1,0:T(8,128)(2,1)S(1)}, bf16[128,2048]{1,0:T(8,128)(2,1)}, u32[]{:S(2)}) copy-start(bf16[128,2048]{1,0:T(8,128)(2,1)} %param.18) | copy-start | bytes 1572868
  129.9 8.2 %slice-start = ((s8[8388608]{0:T(1024)(128)(4,1)}), s8[4194304]{0:T(1024)(128)(4,1)S(1)}, s32[]{:S(2)}) async-start(s8[8388608]{0:T(1024)(128)(4,1)} %bitcast.110), calls=%async_computation.7 | async-start | bytes 8388608 | tf_op jit(solution)/shard_map/cond/branch_1_fun/while
  132.1 6.0 %slice-start.1 = ((s8[8388608]{0:T(1024)(128)(4,1)}), s8[4194304]{0:T(1024)(128)(4,1)S(1)}, s32[]{:S(2)}) async-start(s8[8388608]{0:T(1024)(128)(4,1)} %bitcast.110), calls=%async_computation.8 | async-start | bytes 8388608 | tf_op jit(solution)/shard_map/cond/branch_1_fun/while
  150.8 8.2 %slice-start = ((s8[8388608]{0:T(1024)(128)(4,1)}), s8[4194304]{0:T(1024)(128)(4,1)S(1)}, s32[]{:S(2)}) async-start(s8[8388608]{0:T(1024)(128)(4,1)} %bitcast.110), calls=%async_computation.7 | async-start | bytes 8388608 | tf_op jit(solution)/shard_map/cond/branch_1_fun/while
  152.9 6.1 %slice-start.1 = ((s8[8388608]{0:T(1024)(128)(4,1)}), s8[4194304]{0:T(1024)(128)(4,1)S(1)}, s32[]{:S(2)}) async-start(s8[8388608]{0:T(1024)(128)(4,1)} %bitcast.110), calls=%async_computation.8 | async-start | bytes 8388608 | tf_op jit(solution)/shard_map/cond/branch_1_fun/while
  162.9 8.5 %copy-start.7 = (f32[2048]{0:T(1024)S(1)}, f32[2048]{0:T(1024)}, u32[]{:S(2)}) copy-start(f32[2048]{0:T(1024)} %param.26) | copy-start | bytes 24580
  254.6 16.9 %copy-start.9 = (bf16[1,2048,256]{2,1,0:T(8,128)(2,1)S(1)}, bf16[1,2048,256]{2,1,0:T(8,128)(2,1)}, u32[]{:S(2)}) copy-start(bf16[1,2048,256]{2,1,0:T(8,128)(2,1)} %param.30) | copy-start | bytes 3145732
  254.6 38.9 %reduce-scatter.2.cloned.1.call-start = ((), (), s32[]{:S(2)}) async-start(), calls=%async_computation.6 | async-start | bytes 6291456 | tf_op jit(solution)/shard_map/reduce_scatter | solution.py:186
  280.0 20.5 %copy-start.8 = (f32[128,2]{0,1:T(2,128)S(1)}, f32[128,2]{0,1:T(2,128)}, u32[]{:S(2)}) copy-start(f32[128,2]{0,1:T(2,128)} %param.28) | copy-start | bytes 3076
  293.5 55.4 %all-to-all-start.2 = ((bf16[16,32,2048]{2,1,0:T(8,128)(2,1)}), bf16[16,32,2048]{2,1,0:T(8,128)(2,1)S(1)}, u32[]{:S(2)}, u32[]{:S(2)}) async-start(bf16[16,32,2048]{2,1,0:T(8,128)(2,1)} %reduce-scatter.2.cloned.1.call-done), calls=%async_computation.3 | async-start | bytes 4194304 | tf_op jit(solution)/shard_map/all_to_all | solution.py:194
  351.2 8.2 %copy-start.2 = (f32[128,2048]{1,0:T(8,128)S(1)}, f32[128,2048]{1,0:T(8,128)}, u32[]{:S(2)}) copy-start(f32[128,2048]{1,0:T(8,128)} %copy-done.1) | copy-start | bytes 3145732
  (5 other events, 12.6 us)
Sparse Core Ops, SparseCore 0:
  29.0 69.5 all-gather.2
  254.7 12.9 all-gather.4
  280.1 13.2 reduce-scatter.1
